TPU v7x, 32 devices: a whole 2x2x4 slice. The times are simulated.
32 devices in a mesh: sp: 4 (over z), dp: 8 (over y, x, core).
Axes of the slice: x: 2, y: 2, z: 4, core: 2. Of those that a mesh axis runs over, the one named last changes fastest.
Arguments:
- queries: bfloat16 [8, 768, 1024], P('dp', 'sp'), may hold values from -6 to 6
- keys: bfloat16 [8, 768, 256], P('dp', 'sp'), may hold values from -6 to 6
- values: bfloat16 [8, 768, 256], P('dp', 'sp'), may hold values from -6 to 6
- query_gain: float32 [64], replicated, may hold values from 0.15 to 7
- key_gain: float32 [64], replicated, may hold values from 0.15 to 7
- out_weight: bfloat16 [1024, 2048], P(None, 'dp'), may hold values from -0.1875 to 0.1875
- out_gain: float32 [2048], replicated, may hold values from 0.1 to 1.9
Outputs:
- output: bfloat16 [8, 768, 2048], P('dp', 'sp')
All inputs are finite; a program needn't handle non-finite values.
Results may differ from a plain program's by a relative error of at most 0.0035.
The roundings to bfloat16 on the way count: a program that leaves them out, or rounds other values in their place, can miss the bound.
Values may be sent and summed in bfloat16 or wider, within the bound.
A program may use at most 64 MiB of HBM per device.

v0:
```python
import functools

import jax
import jax.numpy as jnp
import numpy as np
from jax import lax
from jax.experimental import pallas as pl
from jax.experimental.pallas import tpu as pltpu
from jax.sharding import PartitionSpec as P

QH = 16
KVH = 4
HEAD = 64
GRID_W = 64
GROUP = QH // KVH
HALVES = 2
BLOCK = GROUP * HEAD
WIDTH = 128

TO_END = 128
TO_INNER = 160
CHUNKS = (256, 128, 128)
LATE = 128
PIECES = 8 * len(CHUNKS) + 17


EPSILON = 1e-06
ROTARY_BASE = 10000.0

F32 = jnp.float32
BF16 = jnp.bfloat16


def rotate(vectors, positions, width):
    half_width = width // 2
    frequency = ROTARY_BASE ** (-jnp.arange(0, width, 2, dtype=jnp.float32) / width)
    angles = positions.astype(jnp.float32)[:, None] * frequency[None, :]
    cosines = jnp.cos(angles)[:, None, :]
    sine_table = jnp.sin(angles)[:, None, :]
    first_half = vectors[..., :half_width]
    second_half = vectors[..., half_width:]
    return jnp.concatenate(
        [
            first_half * cosines - second_half * sine_table,
            second_half * cosines + first_half * sine_table,
        ],
        axis=-1,
    )


def prepare(vectors, gain_vector, grid_row, grid_col):
    vectors = vectors.astype(jnp.float32)
    vectors = (
        vectors
        * lax.rsqrt(jnp.mean(vectors * vectors, axis=-1, keepdims=True) + EPSILON)
        * gain_vector
    )
    half_width = HEAD // 2
    turned = jnp.concatenate(
        [
            rotate(vectors[..., :half_width], grid_row, half_width),
            rotate(vectors[..., half_width:], grid_col, half_width),
        ],
        axis=-1,
    )
    return turned.astype(jnp.bfloat16)


def softmax_rows(scores):
    row_max = jnp.max(scores, axis=-1, keepdims=True)
    exponent = jnp.exp(scores - row_max)
    return exponent / jnp.sum(exponent, axis=-1, keepdims=True)


def per_device_general(queries, keys, values, query_gain, key_gain, out_weight, out_gain):
    sp_count = lax.axis_size("sp")
    tokens_here = queries.shape[1]
    seq_len = tokens_here * sp_count
    score_scale = HEAD ** (-0.5)
    offset = lax.axis_index("sp") * tokens_here
    positions = offset + jnp.arange(tokens_here, dtype=jnp.int32)
    grid_row = positions // GRID_W
    grid_col = positions % GRID_W
    query_rot = prepare(queries[0].reshape(tokens_here, QH, HEAD), query_gain, grid_row, grid_col)
    key_rot = prepare(keys[0].reshape(tokens_here, KVH, HEAD), key_gain, grid_row, grid_col)
    value_heads = values[0].reshape(tokens_here, KVH, HEAD)
    kv_pairs = jnp.concatenate([key_rot, value_heads], axis=2)
    all_pairs = lax.all_gather(
        kv_pairs.reshape(tokens_here, KVH * 2 * HEAD), "sp", axis=0, tiled=True
    )
    all_pairs = all_pairs.reshape(seq_len, KVH, 2, HEAD)
    key_all = all_pairs[:, :, 0].transpose(1, 0, 2)
    value_all = all_pairs[:, :, 1].transpose(1, 0, 2)
    query_groups = query_rot.reshape(tokens_here, KVH, QH // KVH, HEAD).transpose(1, 0, 2, 3)

    def attend_group(operands):
        query_group, key_head, value_head = operands
        scores = (
            jnp.einsum("qgd,kd->gqk", query_group, key_head, preferred_element_type=jnp.float32)
            * score_scale
        )
        attn_weights = softmax_rows(scores).astype(jnp.bfloat16)
        return jnp.einsum(
            "gqk,kd->qgd", attn_weights, value_head, preferred_element_type=jnp.float32
        ).astype(jnp.bfloat16)

    results = lax.map(attend_group, (query_groups, key_all, value_all))
    attended = results.transpose(1, 0, 2, 3).reshape(tokens_here, QH * HEAD)
    projected = jnp.dot(
        attended,
        lax.all_gather(out_weight, "dp", axis=1, tiled=True),
        preferred_element_type=jnp.float32,
    )
    normed = (
        projected
        * lax.rsqrt(jnp.mean(projected * projected, axis=-1, keepdims=True) + EPSILON)
        * out_gain
    )
    return normed.astype(jnp.bfloat16)[None]


def position_tables(seq_len):
    width = HEAD // 2
    frequency = np.float32(ROTARY_BASE) ** (
        -np.arange(0, width, 2, dtype=np.float32) / np.float32(width)
    )
    position = np.arange(seq_len)
    parts = []
    for coordinate in (position // GRID_W, position % GRID_W):
        angles = coordinate.astype(np.float32)[:, None] * frequency[None, :]
        parts += [angles, angles]
    angles = np.concatenate(parts * 2, axis=1).astype(np.float64)
    return np.stack([np.cos(angles), np.sin(angles)]).astype(np.float32)


def dot(a, b):
    return jnp.dot(a, b, preferred_element_type=F32)


def cross(a, b):
    return lax.dot_general(a, b, (((1,), (1,)), ((), ())), preferred_element_type=F32)


def kernel(
    sp, dp,
    q_ref, k_ref, v_ref, qg_hbm, kg_hbm, w_ref, og_hbm, table_ref,
    out_ref,
    q_raw, k_all, v_all, tables, w_all, gains,
    swap_mat, ones_mat, q_t, v_turned, v_last, partial,
    expo, peak, total, mixed, att, proj,
    qg_ref, kg_ref, og_ref, local_sem, kv_send, kv_recv, w_send, w_recv,
):
    tokens = q_raw.shape[0]
    depth = w_ref.shape[0]
    half = depth // 2
    me = lax.axis_index("sp")
    here = lax.axis_index("dp")
    mate = here + 1 - 2 * (here % 2)
    flip_x = 2 - 4 * ((here // 2) % 2)
    flip_y = 4 - 8 * ((here // 4) % 2)
    dev_x = here + flip_x
    dev_y = here + flip_y
    dev_d = here + flip_x + flip_y

    barrier = pltpu.get_barrier_semaphore()
    has_left = me > 0
    has_right = me < sp - 1

    for other in (mate, dev_x, dev_y):
        pl.semaphore_signal(barrier, inc=1, device_id={"dp": other})

    @pl.when(has_left)
    def _():
        pl.semaphore_signal(barrier, inc=1, device_id={"sp": me - 1})

    @pl.when(has_right)
    def _():
        pl.semaphore_signal(barrier, inc=1, device_id={"sp": me + 1})

    locals_ = [
        pltpu.make_async_copy(k_ref, k_all.at[pl.ds(me * tokens, tokens)], local_sem.at[0]),
        pltpu.make_async_copy(v_ref, v_all.at[pl.ds(me * tokens, tokens)], local_sem.at[1]),
        pltpu.make_async_copy(w_ref, w_all.at[here], local_sem.at[2]),
        pltpu.make_async_copy(q_ref, q_raw, local_sem.at[3]),
        pltpu.make_async_copy(table_ref, tables, local_sem.at[4]),
        pltpu.make_async_copy(qg_hbm, qg_ref, local_sem.at[5]),
        pltpu.make_async_copy(kg_hbm, kg_ref, local_sem.at[6]),
        pltpu.make_async_copy(og_hbm, og_ref, local_sem.at[7]),
    ]
    for copy in locals_:
        copy.start()

    row_id = lax.broadcasted_iota(jnp.int32, (BLOCK, BLOCK), 0)
    col_id = lax.broadcasted_iota(jnp.int32, (BLOCK, BLOCK), 1)
    quarter = HEAD // 4
    second = (col_id & (HEAD // 2 - 1)) >= quarter
    partner_col = jnp.where(second, col_id - quarter, col_id + quarter)
    hit = row_id == partner_col
    swap_mat[...] = jnp.where(hit, jnp.where(second, 1.0, -1.0), 0.0).astype(BF16)
    ones_mat[...] = jnp.where((row_id // HEAD) == (col_id // HEAD), 1.0, 0.0).astype(BF16)
    spread = jnp.where(
        row_id[:HEAD] == (col_id[:HEAD] & (HEAD - 1)), 1.0, 0.0
    ).astype(BF16)
    spread_swapped = jnp.where(
        row_id[:HEAD] == (partner_col[:HEAD] & (HEAD - 1)), 1.0, 0.0
    ).astype(BF16)
    lane_head = lax.broadcasted_iota(jnp.int32, (1, BLOCK), 1) // HEAD
    masks = [jnp.where(lane_head == p, 1.0, 0.0).astype(BF16) for p in range(GROUP)]

    pl.semaphore_wait(barrier, 3 + jnp.minimum(me, 1) + jnp.minimum(sp - 1 - me, 1))

    part = k_ref.shape[1] // HALVES

    stores = (k_all, v_all)
    owns = (k_ref, v_ref)

    def kv_copy(way, step, kind, side):
        block = me - step if way == 0 else me + step
        target = me + 1 if way == 0 else me - 1
        columns = pl.ds(side * part, part)
        window = stores[kind].at[pl.ds(block * tokens, tokens), columns]
        return pltpu.make_async_remote_copy(
            src_ref=owns[kind].at[:, columns] if step == 0 else window,
            dst_ref=window,
            send_sem=kv_send.at[way, step, side, kind],
            recv_sem=kv_recv.at[way, step, side, kind],
            device_id={"sp": target},
        )

    def kv_sends(way, step):
        if way == 0:
            return jnp.logical_and(has_right, me - step >= 0)
        return jnp.logical_and(has_left, me + step < sp)

    def kv_start(way, step, kind, side):
        @pl.when(kv_sends(way, step))
        def _():
            kv_copy(way, step, kind, side).start()

    def kv_arrive(step, kind, side):
        for way in (0, 1):
            source = me - 1 - step if way == 0 else me + 1 + step
            arrives = source >= 0 if way == 0 else source < sp

            @pl.when(arrives)
            def _(way=way, source=source):
                window = stores[kind].at[
                    pl.ds(source * tokens, tokens), pl.ds(side * part, part)
                ]
                pltpu.make_async_remote_copy(
                    src_ref=window,
                    dst_ref=window,
                    send_sem=kv_send.at[way, step, side, kind],
                    recv_sem=kv_recv.at[way, step, side, kind],
                    device_id={"sp": me},
                ).wait_recv()

            if step + 1 < sp - 1:
                kv_start(way, step + 1, kind, side)

    for kind in (0, 1):
        for side in range(HALVES):
            for way in (1, 0):
                kv_start(way, 0, kind, side)

    odd = me % 2
    zmate = me + 1 - 2 * odd
    inner = (me + 1) // 2 % 2 == 1
    outer = jnp.logical_not(inner)
    shares = ((inner, 0, TO_END), (outer, half - TO_INNER, TO_INNER))
    mate_x, mate_y, mate_d = mate + flip_x, mate + flip_y, mate + flip_x + flip_y

    starts = [sum(CHUNKS[:j]) for j in range(len(CHUNKS))]
    pieces = {"own": (mate, 0, depth)}
    for j, (start, size) in enumerate(zip(starts, CHUNKS)):
        pieces["x", j] = (dev_x, half + start, size)
        pieces["y", j] = (dev_y, start, size)
        pieces["dx", j] = (dev_d, start, size)
        pieces["dy", j] = (dev_d, half + start, size)
    for name, shard, base in (("x", dev_x, 0), ("y", dev_y, half)):
        pieces[name, "middle"] = (shard, base + TO_END, half - TO_END - TO_INNER)
        for role, (_, start, size) in enumerate(shares):
            pieces[name, "share", role] = (shard, base + start, size)
    across = {"x": mate_x, "y": mate_y, "dx": mate_d, "dy": mate_d}
    for name in [name for name in pieces if name != "own"]:
        start, size = pieces[name][1:]
        pieces["mate", name] = (across[name[0]], start, size)
        if name[1] == "share":
            pieces["zed", name] = pieces[name]
    order = {name: i for i, name in enumerate(pieces)}
    sent = []

    def w_copy(name, shard, start, size, target, own=False):
        window = w_all.at[shard, pl.ds(start, size)]
        return pltpu.make_async_remote_copy(
            src_ref=w_ref.at[pl.ds(start, size)] if own else window,
            dst_ref=window,
            send_sem=w_send.at[order[name]],
            recv_sem=w_recv.at[order[name]],
            device_id=target,
        )

    def w_give(name, shard, start, size, target, own=False):
        copy = w_copy(name, shard, start, size, target, own)
        copy.start()
        sent.append(copy)

    def w_own(name, target):
        w_give(name, here, *pieces[name][1:], {"dp": target}, own=True)

    def w_wait(name):
        w_copy(name, *pieces[name], {"dp": mate}).wait_recv()

    def w_take(name):
        w_wait(name)
        piece = pieces[name]
        if name[1] in range(len(CHUNKS)):
            if name[0] == "x":
                w_give(("dy", name[1]), *piece, {"dp": dev_y})
            if name[0] == "y":
                w_give(("dx", name[1]), *piece, {"dp": dev_x})
        w_give(("mate", name), *piece, {"dp": mate})

    def w_share_own(name):
        for role, (chosen, _, _) in enumerate(shares):
            @pl.when(chosen)
            def _(key=(name, "share", role)):
                target = dev_x if name == "x" else dev_y
                w_copy(key, here, *pieces[key][1:], {"dp": target}, own=True).start()

    def w_share_near(role):
        @pl.when(shares[role][0])
        def _():
            for name in ("x", "y"):
                key = (name, "share", role)
                w_wait(key)
                w_copy(("zed", key), *pieces[key], {"sp": zmate}).start()
                w_copy(("mate", key), *pieces[key], {"dp": mate}).start()

    def w_share_far(role):
        @pl.when(shares[1 - role][0])
        def _():
            for name in ("x", "y"):
                key = (name, "share", role)
                w_wait(("zed", key))
                w_copy(("mate", key), *pieces[key], {"dp": mate}).start()

    def w_share_sent(name):
        for role, (chosen, _, _) in enumerate(shares):
            key = (name, "share", role)
            w_copy(("mate", key), *pieces[key], {"dp": mate}).wait_send()

            @pl.when(chosen)
            def _(key=key):
                for form in (key, ("zed", key)):
                    w_copy(form, *pieces[key], {"dp": mate}).wait_send()

    for j in range(len(CHUNKS)):
        w_own(("x", j), dev_x)
        w_own(("y", j), dev_y)
    w_share_own("x")
    w_share_own("y")
    w_own(("x", "middle"), dev_x)
    w_own(("y", "middle"), dev_y)
    w_own("own", mate)

    def turned(x, rows, which, scale):
        xf = x.astype(F32)
        square = xf * xf
        high = square.astype(BF16)
        low = (square - high.astype(F32)).astype(BF16)
        size = x.shape[1]
        ones = ones_mat[:size, :size]
        mean = (dot(high, ones) + dot(low, ones)) * (1.0 / HEAD)
        inverse = lax.rsqrt(mean + EPSILON) * scale
        swapped = dot(x, swap_mat[:size, :size])
        cosines = tables[0, rows, :]
        sines = tables[1, rows, :]
        if size > 2 * HEAD:
            cosines = jnp.concatenate([cosines, cosines], axis=1)
            sines = jnp.concatenate([sines, sines], axis=1)
        cosines = cosines * gains[2 * which, 0:1, :size]
        sines = sines * gains[2 * which + 1, 0:1, :size]
        return ((xf * cosines + swapped * sines) * inverse).astype(BF16)

    locals_[5].wait()
    locals_[6].wait()
    for i, gain_ref in enumerate((qg_ref, kg_ref)):
        gain = jnp.broadcast_to(gain_ref[...], (16, HEAD))
        first = gain.astype(BF16)
        rest = gain - first.astype(F32)
        mid = rest.astype(BF16)
        low = (rest - mid.astype(F32)).astype(BF16)
        for j, matrix in enumerate((spread, spread_swapped)):
            gains[2 * i + j] = (dot(first, matrix) + dot(mid, matrix)) + dot(low, matrix)

    locals_[3].wait()
    locals_[4].wait()
    locals_[7].wait()
    own_rows = pl.ds(pl.multiple_of(me * tokens, 64), tokens)
    for b in range(KVH):
        columns = slice(b * BLOCK, (b + 1) * BLOCK)
        query = turned(q_raw[:, columns], own_rows, 0, HEAD ** (-0.5))
        parts = [query[:WIDTH] * mask for mask in masks] + [query[WIDTH:] * mask for mask in masks]
        held = b % 2 * HEAD
        fold = jnp.where(row_id[:part] - held == (col_id[:part] & (HEAD - 1)), 1.0, 0.0)
        q_t[b] = cross(fold.astype(BF16), jnp.concatenate(parts, axis=0)).astype(BF16)

    eye = jnp.where(row_id == col_id, 1.0, 0.0).astype(BF16)
    far = 1 - me // 2
    blocks = [me, zmate, far + 1, 3 * far][:sp]
    spans = [pl.ds(pl.multiple_of(block * tokens, 64), tokens) for block in blocks]
    heads = KVH // HALVES
    rest = tokens - WIDTH
    final = sp - 1

    def score(turn, side):
        lanes = slice(side * part, (side + 1) * part)
        rows = spans[turn]
        key_side = turned(k_all[rows, lanes], rows, 1, 1.0)
        for b in range(side * heads, (side + 1) * heads):
            scores = dot(key_side, q_t[b])
            high = jnp.max(scores, axis=0, keepdims=True)
            if turn < final:
                weights = jnp.exp(scores - high)
                expo[turn, b] = weights
                peak[turn, b] = high
                total[turn, b] = jnp.sum(weights, axis=0, keepdims=True)
                continue
            for t in range(turn):
                high = jnp.maximum(high, peak[t, b])
            weights = jnp.exp(scores - high)
            norm = jnp.sum(weights, axis=0, keepdims=True)
            keeps = [jnp.exp(peak[t, b] - high) for t in range(turn)]
            for t in range(turn):
                norm = norm + total[t, b] * keeps[t]
            inverse = 1.0 / norm
            for t in range(turn):
                mixed[b, t * tokens : (t + 1) * tokens, :] = (
                    expo[t, b] * (keeps[t] * inverse)
                ).astype(BF16)
            mixed[b, turn * tokens :, :] = (weights * inverse).astype(BF16)

    def values(blocks, side):
        lanes = slice(side * part, (side + 1) * part)
        stack = jnp.concatenate([v_all[spans[t], lanes] for t in blocks], axis=0)
        result = cross(eye[:part, :part], stack).astype(BF16)
        if blocks[0] == final:
            v_last[lanes, :] = result
        else:
            v_turned[lanes, blocks[0] * tokens : (blocks[-1] + 1) * tokens] = result

    def each_head(side):
        for b in range(side * heads, (side + 1) * heads):
            yield b, slice(b * HEAD, (b + 1) * HEAD)

    def early(side):
        for b, value_rows in each_head(side):
            partial[b] = dot(v_turned[value_rows, :], mixed[b, : final * tokens, :])

    def gather(side):
        for b, value_rows in each_head(side):
            product = partial[b] + dot(v_last[value_rows, :], mixed[b, final * tokens :, :])
            for p in range(0, GROUP, 2):
                lanes = slice(b * BLOCK + p * HEAD, b * BLOCK + (p + 2) * HEAD)
                two = [product[:, i * WIDTH : (i + 1) * WIDTH] for i in (p, p + 1)]
                att[:WIDTH, lanes] = jnp.concatenate(two, axis=0).T.astype(BF16)
                start = GROUP * WIDTH + p * rest
                two = product[:, start : start + 2 * rest].T
                two = jnp.concatenate([two[:rest], two[rest:]], axis=1)
                att[WIDTH:, lanes] = two.astype(BF16)

    lots = len(CHUNKS)
    columns_each = w_ref.shape[1]
    late = LATE
    tails = {2: [0], 3: [half], 4: [0], 5: [half]}
    tails[6] = tails[7] = [half - late, depth - late]

    def columns_of(shard):
        return pl.ds(pl.multiple_of(shard * columns_each, columns_each), columns_each)

    def product(shard, start, size):
        rows = pl.ds(start, size)
        return dot(att[:, rows], w_all[shard, rows, :])

    def squares_of(result):
        square = result * result
        return sum(square[:, i : i + 128] for i in range(0, columns_each, 128))

    slots = [here, mate, dev_x, dev_y, mate_x, mate_y, dev_d, mate_d]

    def project(slot, squares):
        shard = slots[slot]
        result = dot(att[...], w_all[shard])
        proj[slot] = result * og_ref[:, columns_of(shard)]
        return squares + squares_of(result)

    def begin(slot):
        done, result = 0, 0.0
        for start in [*tails[slot], depth]:
            if start > done:
                result = result + product(slots[slot], done, start - done)
            done = start + late
        proj[slot] = result

    def end(slot):
        result = proj[slot]
        for start in tails[slot]:
            result = result + product(slots[slot], start, late)
        return result

    def end_early(slot, squares):
        result = end(slot)
        proj[slot] = result * og_ref[:, columns_of(slots[slot])]
        return squares + squares_of(result)

    def take(*names):
        for name in names:
            w_take(("x", name))
            w_take(("y", name))

    def take_far(j):
        w_take(("dx", j))
        w_take(("dy", j))

    locals_[0].wait()
    for side in range(HALVES):
        score(0, side)
    locals_[1].wait()

    jobs = {
        (0, 1, 0): lambda: take(0),
        (0, 1, 1): lambda: take(1),
        (1, 0, 0): lambda: take(*range(2, lots)),
        (1, 1, 0): lambda: w_share_near(1),
        (1, 1, 1): lambda: w_share_near(0),
        (2, 0, 0): lambda: take("middle"),
    }
    for step in range(sp - 1):
        turn = step + 1
        for kind in (0, 1):
            for side in range(HALVES):
                kv_arrive(step, kind, side)
                if kind == 0:
                    score(turn, side)
                    if turn == final:
                        if turn == 1:
                            values([0], side)
                        early(side)
                elif turn == final:
                    values([final], side)
                    gather(side)
                    if side == 0:
                        take_far(0)
                elif turn == 1:
                    values([0, 1], side)
                else:
                    values([turn], side)
                if (step, kind, side) in jobs:
                    jobs.pop((step, kind, side))()
    for job in jobs.values():
        job()

    w_share_far(1)
    locals_[2].wait()
    squares = project(0, jnp.zeros((tokens, 128), F32))
    w_wait("own")
    squares = project(1, squares)
    begin(2)
    begin(3)
    for j in range(1, lots - 1):
        take_far(j)
    for slot, name in ((4, "x"), (5, "y")):
        for piece in (*range(lots), "middle"):
            w_wait(("mate", (name, piece)))
        w_wait(("mate", (name, "share", 1)))
        begin(slot)
    begin(6)
    w_share_far(0)
    take_far(lots - 1)
    for slot in (2, 3):
        squares = end_early(slot, squares)
    for j in range(lots - 1):
        w_wait(("mate", ("dx", j)))
        w_wait(("mate", ("dy", j)))
    begin(7)
    for slot, name in ((4, "x"), (5, "y")):
        w_wait(("mate", (name, "share", 0)))
        squares = end_early(slot, squares)
    for axis in ("dx", "dy"):
        w_wait(("mate", (axis, lots - 1)))
    ends = [end(6), end(7)]
    for result in ends:
        squares = squares + squares_of(result)
    squares = jnp.sum(squares, axis=1, keepdims=True)
    inverse = lax.rsqrt(squares * (1.0 / (columns_each * dp)) + EPSILON)
    for slot, shard in enumerate(slots):
        columns = columns_of(shard)
        if slot < 6:
            result = proj[slot]
        else:
            result = ends[slot - 6] * og_ref[:, columns]
        out_ref[:, columns] = (result * inverse).astype(BF16)

    for copy in sent:
        copy.wait_send()
    for name in ("x", "y"):
        w_share_sent(name)
    for step in range(sp - 1):
        for way in (0, 1):
            @pl.when(kv_sends(way, step))
            def _(way=way, step=step):
                for kind in (0, 1):
                    for side in range(HALVES):
                        kv_copy(way, step, kind, side).wait_send()


def per_device_fused(sp, dp, queries, keys, values, query_gain, key_gain, out_weight, out_gain):
    tokens = queries.shape[1]
    depth, columns = out_weight.shape
    hidden = queries.shape[2]
    kv_width = keys.shape[2]
    seq_len = tokens * sp
    hbm_spec = pl.BlockSpec(memory_space=pltpu.HBM)
    vmem_spec = pl.BlockSpec(memory_space=pltpu.VMEM)
    result = pl.pallas_call(
        functools.partial(kernel, sp, dp),
        out_shape=pltpu.VMEM((tokens, columns * dp), BF16),
        in_specs=[hbm_spec] * 8,
        out_specs=vmem_spec,
        scratch_shapes=[
            pltpu.VMEM((tokens, hidden), BF16),
            pltpu.VMEM((seq_len, kv_width), BF16),
            pltpu.VMEM((seq_len, kv_width), BF16),
            pltpu.VMEM((2, seq_len, 2 * HEAD), F32),
            pltpu.VMEM((dp, depth, columns), BF16),
            pltpu.VMEM((4, 16, BLOCK), F32),
            pltpu.VMEM((BLOCK, BLOCK), BF16),
            pltpu.VMEM((BLOCK, BLOCK), BF16),
            pltpu.VMEM((KVH, kv_width // HALVES, GROUP * tokens), BF16),
            pltpu.VMEM((kv_width, seq_len - tokens), BF16),
            pltpu.VMEM((kv_width, tokens), BF16),
            pltpu.VMEM((KVH, HEAD, GROUP * tokens), F32),
            pltpu.VMEM((sp - 1, KVH, tokens, GROUP * tokens), F32),
            pltpu.VMEM((sp - 1, KVH, 1, GROUP * tokens), F32),
            pltpu.VMEM((sp - 1, KVH, 1, GROUP * tokens), F32),
            pltpu.VMEM((KVH, seq_len, GROUP * tokens), BF16),
            pltpu.VMEM((tokens, hidden), BF16),
            pltpu.VMEM((dp, tokens, columns), F32),
            pltpu.VMEM((1, HEAD), F32),
            pltpu.VMEM((1, HEAD), F32),
            pltpu.VMEM((1, columns * dp), F32),
            pltpu.SemaphoreType.DMA((8,)),
            pltpu.SemaphoreType.DMA((2, sp - 1, HALVES, 2)),
            pltpu.SemaphoreType.DMA((2, sp - 1, HALVES, 2)),
            pltpu.SemaphoreType.DMA((PIECES,)),
            pltpu.SemaphoreType.DMA((PIECES,)),
        ],
        compiler_params=pltpu.CompilerParams(
            collective_id=0, has_side_effects=True, vmem_limit_bytes=66000000
        ),
    )(
        queries[0], keys[0], values[0], query_gain[None], key_gain[None],
        out_weight, out_gain[None], jnp.asarray(position_tables(seq_len)),
    )
    return result[None]


def solution(mesh):
    sp, dp = mesh.shape["sp"], mesh.shape["dp"]
    if dp == 8 and sp >= 2 and sp % 2 == 0 and sp <= 4:
        body = functools.partial(per_device_fused, sp, dp)
    else:
        body = per_device_general
    return jax.shard_map(
        body,
        mesh=mesh,
        in_specs=(
            P("dp", "sp", None),
            P("dp", "sp", None),
            P("dp", "sp", None),
            P(),
            P(),
            P(None, "dp"),
            P(),
        ),
        out_specs=P("dp", "sp", None),
        check_vma=False,
    )
```

profile of v0, /device:TPU:1, one launch (start us, length us, event | category | flops | bytes accessed | tf_op | source)
XLA Modules:
  0.0 24.7 jit_solution(12443225203609605404)
XLA Ops:
  0.0 23.8 %shard_map.82 = bf16[192,2048]{1,0:T(8,128)(2,1)S(1)} custom-call(bf16[192,1024]{1,0:T(8,128)(2,1)} %bitcast.8, bf16[192,256]{1,0:T(8,128)(2,1)} %bitcast.9, bf16[192,256]{1,0:T(8,128)(2,1)} %bitcast.10, f32[1,64]{1,0:T(1,128)} %bitcast.12, f32[1,64]{1,0:T(1,128)} %bitcast.13, bf16[1024,256]{1,0:T(8,128)(2,1)} %w_ref.1, f32[1,2048]{1,0:T(1,128)} %bitcast.11, ...), custom_call_target="tpu_custom_call" | custom-call | tf_op jit(solution)/shard_map/pallas_call | solution.py:626
  23.8 0.9 %copy.10 = bf16[1,192,2048]{2,1,0:T(8,128)(2,1)} copy(bf16[1,192,2048]{2,1,0:T(8,128)(2,1)S(1)} %bitcast.7) | data formatting | bytes 1572864
where the time goes:
time: 24.8 us; the launch traced here: 24.7 us
  Pallas kernels  23.8 us (96%)
  local copies, waits for them, and re-layouts  0.88 us (4%)
    pallas_call x1, Pallas kernels, per_device_fused(): pl.pallas_call(functools.partial(kernel, sp, dp), out_shape=pltpu.VMEM((t...  23.8 us
    unnamed x1, local copies, waits for them, and re-layouts  0.88 us

commit v1 on v0

--- a/solution.py
+++ b/solution.py
@@ -18,7 +18,7 @@
 WIDTH = 128
 
 TO_END = 128
-TO_INNER = 160
+TO_INNER = 192
 CHUNKS = (256, 128, 128)
 LATE = 128
 PIECES = 8 * len(CHUNKS) + 17
@@ -148,7 +148,7 @@
     q_raw, k_all, v_all, tables, w_all, gains,
     swap_mat, ones_mat, q_t, v_turned, v_last, partial,
     expo, peak, total, mixed, att, proj,
-    qg_ref, kg_ref, og_ref, local_sem, kv_send, kv_recv, w_send, w_recv,
+    qg_ref, kg_ref, og_ref, above, local_sem, kv_send, kv_recv, w_send, w_recv,
 ):
     tokens = q_raw.shape[0]
     depth = w_ref.shape[0]
@@ -166,16 +166,19 @@
     has_left = me > 0
     has_right = me < sp - 1
 
-    for other in (mate, dev_x, dev_y):
-        pl.semaphore_signal(barrier, inc=1, device_id={"dp": other})
-
-    @pl.when(has_left)
-    def _():
-        pl.semaphore_signal(barrier, inc=1, device_id={"sp": me - 1})
-
-    @pl.when(has_right)
-    def _():
-        pl.semaphore_signal(barrier, inc=1, device_id={"sp": me + 1})
+    low_x, low_y = (here // 2) % 2 == 0, (here // 4) % 2 == 0
+    high_x, high_y = jnp.logical_not(low_x), jnp.logical_not(low_y)
+    ways = (
+        (low_x, high_x, {"dp": dev_x}, {"dp": dev_x}),
+        (low_y, high_y, {"dp": dev_y}, {"dp": dev_y}),
+        (has_right, has_left, {"sp": me + 1}, {"sp": me - 1}),
+    )
+
+    pl.semaphore_signal(barrier, inc=1, device_id={"dp": mate})
+    for up, _, target, _ in ways:
+        @pl.when(up)
+        def _(target=target):
+            pl.semaphore_signal(barrier, inc=1, device_id=target)
 
     locals_ = [
         pltpu.make_async_copy(k_ref, k_all.at[pl.ds(me * tokens, tokens)], local_sem.at[0]),
@@ -207,7 +210,12 @@
     lane_head = lax.broadcasted_iota(jnp.int32, (1, BLOCK), 1) // HEAD
     masks = [jnp.where(lane_head == p, 1.0, 0.0).astype(BF16) for p in range(GROUP)]
 
-    pl.semaphore_wait(barrier, 3 + jnp.minimum(me, 1) + jnp.minimum(sp - 1 - me, 1))
+    pl.semaphore_wait(barrier, 1 + (here // 2) % 2 + (here // 4) % 2 + jnp.minimum(me, 1))
+
+    for axis, (_, down, _, target) in enumerate(ways):
+        @pl.when(down)
+        def _(axis=axis, target=target):
+            pl.semaphore_signal(above.at[axis], inc=1, device_id=target)
 
     part = k_ref.shape[1] // HALVES
 
@@ -258,10 +266,6 @@
             if step + 1 < sp - 1:
                 kv_start(way, step + 1, kind, side)
 
-    for kind in (0, 1):
-        for side in range(HALVES):
-            for way in (1, 0):
-                kv_start(way, 0, kind, side)
 
     odd = me % 2
     zmate = me + 1 - 2 * odd
@@ -303,7 +307,7 @@
     def w_give(name, shard, start, size, target, own=False):
         copy = w_copy(name, shard, start, size, target, own)
         copy.start()
-        sent.append(copy)
+        sent.append((name, copy))
 
     def w_own(name, target):
         w_give(name, here, *pieces[name][1:], {"dp": target}, own=True)
@@ -347,22 +351,53 @@
 
     def w_share_sent(name):
         for role, (chosen, _, _) in enumerate(shares):
+            @pl.when(chosen)
+            def _(key=(name, "share", role)):
+                for form in (key, ("zed", key)):
+                    w_copy(form, *pieces[key], {"dp": mate}).wait_send()
+
+    def w_share_done(name):
+        for role in range(len(shares)):
             key = (name, "share", role)
             w_copy(("mate", key), *pieces[key], {"dp": mate}).wait_send()
 
-            @pl.when(chosen)
-            def _(key=key):
-                for form in (key, ("zed", key)):
-                    w_copy(form, *pieces[key], {"dp": mate}).wait_send()
-
-    for j in range(len(CHUNKS)):
-        w_own(("x", j), dev_x)
-        w_own(("y", j), dev_y)
-    w_share_own("x")
-    w_share_own("y")
-    w_own(("x", "middle"), dev_x)
-    w_own(("y", "middle"), dev_y)
+    def settle(names):
+        for name, copy in [item for item in sent if item[0] in names]:
+            copy.wait_send()
+            sent.remove((name, copy))
+
+    def own_list(name):
+        return [(name, j) for j in range(len(CHUNKS))], (name, "middle")
+
+    def w_start(name, target):
+        chunks, middle = own_list(name)
+        for key in chunks:
+            w_copy(key, here, *pieces[key][1:], {"dp": target}, own=True).start()
+        w_share_own(name)
+        w_copy(middle, here, *pieces[middle][1:], {"dp": target}, own=True).start()
+
+    def kv_begin(way):
+        for kind in (0, 1):
+            for side in range(HALVES):
+                kv_copy(way, 0, kind, side).start()
+
+    begins = (
+        (lambda: w_start("x", dev_x),) * 2,
+        (lambda: w_start("y", dev_y),) * 2,
+        (lambda: kv_begin(0), lambda: kv_begin(1)),
+    )
+    for (_, down, _, _), (_, start) in zip(ways, begins):
+        pl.when(down)(start)
+    for name, target in (("x", dev_x), ("y", dev_y)):
+        chunks, middle = own_list(name)
+        for key in [*chunks, middle]:
+            sent.append((key, w_copy(key, here, *pieces[key][1:], {"dp": target}, own=True)))
     w_own("own", mate)
+    for axis, ((up, _, _, _), (start, _)) in enumerate(zip(ways, begins)):
+        @pl.when(up)
+        def _(axis=axis, start=start):
+            pl.semaphore_wait(above.at[axis], 1)
+            start()
 
     def turned(x, rows, which, scale):
         xf = x.astype(F32)
@@ -576,6 +611,16 @@
         w_wait(("mate", (name, "share", 1)))
         begin(slot)
     begin(6)
+    settle([name for name, _ in sent if not {"dx", "dy"} & {name[0], name[1][0] if name[0] == "mate" else ""}])
+    for name in ("x", "y"):
+        w_share_sent(name)
+    for step in range(sp - 1):
+        for way in (0, 1):
+            @pl.when(kv_sends(way, step))
+            def _(way=way, step=step):
+                for kind in (0, 1):
+                    for side in range(HALVES):
+                        kv_copy(way, step, kind, side).wait_send()
     w_share_far(0)
     take_far(lots - 1)
     for slot in (2, 3):
@@ -602,17 +647,9 @@
             result = ends[slot - 6] * og_ref[:, columns]
         out_ref[:, columns] = (result * inverse).astype(BF16)
 
-    for copy in sent:
-        copy.wait_send()
+    settle([name for name, _ in sent])
     for name in ("x", "y"):
-        w_share_sent(name)
-    for step in range(sp - 1):
-        for way in (0, 1):
-            @pl.when(kv_sends(way, step))
-            def _(way=way, step=step):
-                for kind in (0, 1):
-                    for side in range(HALVES):
-                        kv_copy(way, step, kind, side).wait_send()
+        w_share_done(name)
 
 
 def per_device_fused(sp, dp, queries, keys, values, query_gain, key_gain, out_weight, out_gain):
@@ -650,6 +687,7 @@
             pltpu.VMEM((1, HEAD), F32),
             pltpu.VMEM((1, HEAD), F32),
             pltpu.VMEM((1, columns * dp), F32),
+            pltpu.SemaphoreType.REGULAR((3,)),
             pltpu.SemaphoreType.DMA((8,)),
             pltpu.SemaphoreType.DMA((2, sp - 1, HALVES, 2)),
             pltpu.SemaphoreType.DMA((2, sp - 1, HALVES, 2)),

time: 24.8 us -> 24.1 us (0.972)
  Pallas kernels: 23.8 us -> 23.1 us
    pallas_call x1, Pallas kernels: 23.8 us -> 23.1 us  [per_device_fused(): pl.pallas_call(functools.partial(kernel, sp, dp), out_shape=pltpu.VMEM((t...]
where the time goes in v1:
time: 24.1 us; the launch traced here: 23.9 us
  Pallas kernels  23.1 us (96%)
  local copies, waits for them, and re-layouts  0.88 us (4%)
    pallas_call x1, Pallas kernels, per_device_fused(): pl.pallas_call(functools.partial(kernel, sp, dp), out_shape=pltpu.VMEM((t...  23.1 us
    unnamed x1, local copies, waits for them, and re-layouts  0.88 us

profile of v1, /device:TPU:1, one launch (start us, length us, event | category | flops | bytes accessed | tf_op | source)
XLA Modules:
  0.0 23.9 jit_solution(14977116914266931437)
XLA Ops:
  0.0 23.1 %shard_map.82 = bf16[192,2048]{1,0:T(8,128)(2,1)S(1)} custom-call(bf16[192,1024]{1,0:T(8,128)(2,1)} %bitcast.8, bf16[192,256]{1,0:T(8,128)(2,1)} %bitcast.9, bf16[192,256]{1,0:T(8,128)(2,1)} %bitcast.10, f32[1,64]{1,0:T(1,128)} %bitcast.12, f32[1,64]{1,0:T(1,128)} %bitcast.13, bf16[1024,256]{1,0:T(8,128)(2,1)} %w_ref.1, f32[1,2048]{1,0:T(1,128)} %bitcast.11, ...), custom_call_target="tpu_custom_call" | custom-call | tf_op jit(solution)/shard_map/pallas_call | solution.py:663
  23.1 0.9 %copy.10 = bf16[1,192,2048]{2,1,0:T(8,128)(2,1)} copy(bf16[1,192,2048]{2,1,0:T(8,128)(2,1)S(1)} %bitcast.7) | data formatting | bytes 1572864

commit v2 on v1

--- a/solution.py
+++ b/solution.py
@@ -585,8 +585,6 @@
                 elif turn == final:
                     values([final], side)
                     gather(side)
-                    if side == 0:
-                        take_far(0)
                 elif turn == 1:
                     values([0, 1], side)
                 else:
@@ -596,6 +594,7 @@
     for job in jobs.values():
         job()
 
+    take_far(0)
     w_share_far(1)
     locals_[2].wait()
     squares = project(0, jnp.zeros((tokens, 128), F32))

time: 24.1 us -> 24.1 us (level)
  no operation moved by 1% of the time
where the time goes in v2:
time: 24.1 us; the launch traced here: 23.9 us
  Pallas kernels  23.1 us (96%)
  local copies, waits for them, and re-layouts  0.88 us (4%)
    pallas_call x1, Pallas kernels, per_device_fused(): pl.pallas_call(functools.partial(kernel, sp, dp), out_shape=pltpu.VMEM((t...  23.1 us
    unnamed x1, local copies, waits for them, and re-layouts  0.88 us

profile of v2, /device:TPU:1, one launch (start us, length us, event | category | flops | bytes accessed | tf_op | source)
XLA Modules:
  0.0 23.9 jit_solution(15750066811366216521)
XLA Ops:
  0.0 23.1 %shard_map.82 = bf16[192,2048]{1,0:T(8,128)(2,1)S(1)} custom-call(bf16[192,1024]{1,0:T(8,128)(2,1)} %bitcast.8, bf16[192,256]{1,0:T(8,128)(2,1)} %bitcast.9, bf16[192,256]{1,0:T(8,128)(2,1)} %bitcast.10, f32[1,64]{1,0:T(1,128)} %bitcast.12, f32[1,64]{1,0:T(1,128)} %bitcast.13, bf16[1024,256]{1,0:T(8,128)(2,1)} %w_ref.1, f32[1,2048]{1,0:T(1,128)} %bitcast.11, ...), custom_call_target="tpu_custom_call" | custom-call | tf_op jit(solution)/shard_map/pallas_call | solution.py:662
  23.1 0.9 %copy.10 = bf16[1,192,2048]{2,1,0:T(8,128)(2,1)} copy(bf16[1,192,2048]{2,1,0:T(8,128)(2,1)S(1)} %bitcast.7) | data formatting | bytes 1572864
